TPU v7x, 32 devices: a whole 2x2x4 slice. The times are simulated.
32 devices in a mesh: row: 8 (over z, core), col: 4 (over y, x).
Axes of the slice: x: 2, y: 2, z: 4, core: 2. Of those that a mesh axis runs over, the one named last changes fastest.
Arguments:
- tokens: bfloat16 [4096, 2048], P('row'), may hold values from -6 to 6
- out_weight: bfloat16 [2048, 2048], P(None, 'col'), may hold values from -0.125 to 0.125
Outputs:
- mixed: bfloat16 [4096, 2048], P('row', 'col')
All inputs are finite; a program needn't handle non-finite values.
Results may differ from a plain program's by a relative error of at most 0.001.
Values may be sent and summed in bfloat16 or wider, within the bound.
A program may use at most 64 MiB of HBM per device.

v0:
```python
import math

import functools

import jax
import jax.numpy as jnp
import numpy as np
from jax import lax
from jax.experimental import pallas as pl
from jax.experimental.pallas import tpu as pltpu
from jax.sharding import PartitionSpec as P

GROUPS = 4
GROUP_DIM = 512


def angles(product, period):
    return (product % period).astype(jnp.float32) * (2.0 * math.pi / period)


def plain_dot(matrix, values):
    return jnp.dot(
        matrix, values, precision=lax.Precision.HIGHEST, preferred_element_type=jnp.float32
    )


def whole_transform(whole_rows, row_count, seg_rows, length):
    few_chans = whole_rows.shape[2]
    lattice = jnp.arange(row_count, dtype=jnp.int32)
    phases = angles(lattice[:, None] * lattice[None, :], row_count)
    cosine_table = jnp.cos(phases)
    sine_table = jnp.sin(phases)
    real_in = whole_rows[0].reshape(row_count, seg_rows * few_chans)
    imag_in = whole_rows[1].reshape(row_count, seg_rows * few_chans)
    first_re = (plain_dot(cosine_table, real_in) + plain_dot(sine_table, imag_in)).reshape(
        row_count, seg_rows, few_chans
    )
    first_im = (plain_dot(cosine_table, imag_in) - plain_dot(sine_table, real_in)).reshape(
        row_count, seg_rows, few_chans
    )
    inner = jnp.arange(seg_rows, dtype=jnp.int32)
    twist = angles(lattice[:, None] * inner[None, :], length)[:, :, None]
    twist_cos = jnp.cos(twist)
    twist_sin = jnp.sin(twist)
    turned_re = twist_cos * first_re + twist_sin * first_im
    turned_im = twist_cos * first_im - twist_sin * first_re
    folded_re = jnp.transpose(turned_re, (1, 0, 2)).reshape(seg_rows, row_count * few_chans)
    folded_im = jnp.transpose(turned_im, (1, 0, 2)).reshape(seg_rows, row_count * few_chans)
    seg_phases = angles(inner[:, None] * inner[None, :], seg_rows)
    real_part = plain_dot(jnp.cos(seg_phases), folded_re) + plain_dot(
        jnp.sin(seg_phases), folded_im
    )
    return real_part.reshape(length, few_chans)


def general_body(tokens, out_weight):
    seg_rows = tokens.shape[0]
    col_width = out_weight.shape[1]
    row_count = lax.axis_size("row")
    length = seg_rows * row_count
    scaling = 1.0 / math.sqrt(length * GROUP_DIM)
    weight_wide = out_weight.astype(jnp.float32)
    lattice = jnp.arange(GROUP_DIM, dtype=jnp.int32)
    phases = angles(lattice[:, None] * lattice[None, :], GROUP_DIM)
    cosine_table = jnp.cos(phases) * scaling
    sine_table = jnp.sin(phases) * scaling
    folded_rows = []
    for group in range(GROUPS):
        group_rows = weight_wide[group * GROUP_DIM : (group + 1) * GROUP_DIM]
        folded_rows.append(
            jnp.concatenate(
                [plain_dot(cosine_table, group_rows), -plain_dot(sine_table, group_rows)], axis=1
            )
        )
    folded_map = jnp.concatenate(folded_rows, axis=0)
    spectrum = plain_dot(tokens.astype(jnp.float32), folded_map)
    stacked = jnp.stack([spectrum[:, :col_width], spectrum[:, col_width:]])
    whole_rows = lax.all_to_all(stacked, "row", split_axis=2, concat_axis=1, tiled=True)
    ordered = whole_transform(whole_rows, row_count, seg_rows, length)
    spectral = lax.all_to_all(
        ordered.astype(jnp.bfloat16), "row", split_axis=0, concat_axis=1, tiled=True
    )
    return spectral

RADIX = 8
HALF = 64
LANES = 128
EXTRA = 16
PARTS = 4
CODE = 84.0


def split_table(values):
    big = values.astype(jnp.bfloat16)
    return big, (values - big.astype(np.float64)).astype(jnp.bfloat16)


def tables(size, length):
    index = np.arange(size)
    phase = 2.0 * np.pi * ((index[:, None] * index[None, :]) % size) / size
    high, low = split_table(np.concatenate([np.cos(phase), np.sin(phase)], axis=0))
    turn = 2.0 * np.pi * (index[:, None] * np.arange(RADIX)[None, :]) / length
    twist = np.zeros((size, LANES), np.float32)
    twist[:, :RADIX] = np.cos(turn)
    twist[:, RADIX : 2 * RADIX] = np.sin(turn)
    small = np.arange(RADIX)
    eight = 2.0 * np.pi * ((small[:, None] * small[None, :]) % RADIX) / RADIX
    last = np.concatenate(
        [
            np.repeat(np.cos(eight)[:, :, None], HALF, axis=2),
            np.repeat(np.sin(eight)[:, :, None], HALF, axis=2),
        ],
        axis=2,
    ).astype(np.float32)
    return high, low, twist, last


def dot(a, b):
    return jnp.dot(a, b, preferred_element_type=jnp.float32)


def split(values):
    high = values.astype(jnp.bfloat16)
    return high, (values - high.astype(jnp.float32)).astype(jnp.bfloat16)


def peer_at(step, chip):
    upper = chip // 2
    folded = chip + upper * (3 - 2 * chip)
    place = lax.rem(step + 1 + folded, 4)
    goal = place + place // 2 - 2 * (place // 3)
    return goal + upper * (3 - 2 * goal)


def kernel(
    scaling,
    count,
    tok_hbm,
    w_hbm,
    high_hbm,
    low_hbm,
    twist_ref,
    last_ref,
    out_ref,
    tok_ref,
    w_ref,
    high_ref,
    low_ref,
    tok_s,
    send_a,
    recv_a,
    zhigh,
    zlow,
    turned,
    found_s,
    fold_high,
    fold_low,
    send_b,
    recv_b,
    load_sem,
    send_a_sem,
    recv_a_sem,
    send_b_sem,
    recv_b_sem,
):
    me = lax.axis_index("row")
    chip = me // 2
    chips = count // 2
    size = tok_ref.shape[0]
    groups = tok_ref.shape[1] // size
    inner = size // RADIX
    mid = size // 2
    part_rows = size // PARTS
    loads = []
    for at, (source, target) in enumerate(
        [(high_hbm, high_ref), (low_hbm, low_ref), (tok_hbm, tok_ref)]
    ):
        loads.append(pltpu.make_async_copy(source, target, load_sem.at[at]))

    def load_w(step):
        goal = peer_at(step, chip)
        cols = pl.ds(pl.multiple_of(goal * LANES, LANES), LANES)
        return pltpu.make_async_copy(
            w_hbm.at[:, cols], w_ref.at[:, cols], load_sem.at[3 + step]
        )

    load_w(0).start()
    for load in loads:
        load.start()
    for step in range(1, 4):
        load_w(step).start()
    barrier = pltpu.get_barrier_semaphore()
    for ahead in range(1, count):
        pl.semaphore_signal(
            barrier,
            inc=1,
            device_id={"row": lax.rem(me + ahead, count)},
            device_id_type=pl.DeviceIdType.MESH,
        )

    lane = lax.broadcasted_iota(jnp.int32, (1, LANES), 1)
    first = lane < HALF
    sign = jnp.where(first, 1.0, -1.0)

    def copy_a(part, target):
        return pltpu.make_async_remote_copy(
            src_ref=send_a.at[part, target],
            dst_ref=recv_a.at[part, me],
            send_sem=send_a_sem.at[part, target],
            recv_sem=recv_a_sem.at[part, me],
            device_id={"row": target},
            device_id_type=pl.DeviceIdType.MESH,
        )

    def copy_b(target):
        return pltpu.make_async_remote_copy(
            src_ref=send_b.at[target],
            dst_ref=recv_b.at[me],
            send_sem=send_b_sem.at[target],
            recv_sem=recv_b_sem.at[me],
            device_id={"row": target},
            device_id_type=pl.DeviceIdType.MESH,
        )

    for load in loads[:2]:
        load.wait()

    @pl.loop(0, chips)
    def _(step):
        goal = peer_at(step, chip)
        cols = pl.ds(pl.multiple_of(goal * LANES, LANES), LANES)
        load_w(step).wait()
        side = jnp.concatenate(
            [w_ref[g * size : (g + 1) * size, cols] for g in range(groups)], axis=1
        )
        folded = dot(high_ref[...], side) + dot(low_ref[...], side)

        @pl.when(step == 0)
        def _():
            loads[2].wait()
            place = lax.broadcasted_iota(jnp.int32, (1, size), 1)
            place = (place % RADIX) * inner + place // RADIX
            spot = lax.broadcasted_iota(jnp.int32, (size, size), 0)
            perm = jnp.where(spot == place, 1.0, 0.0).astype(jnp.bfloat16)
            for g in range(groups):
                span = slice(g * size, (g + 1) * size)
                tok_s[:, span] = dot(perm, tok_ref[:, span]).astype(jnp.bfloat16)

        for g in range(groups):
            cosw = folded[:size, g * LANES : (g + 1) * LANES]
            sinw = -folded[size:, g * LANES : (g + 1) * LANES]
            pair = jnp.concatenate(
                [
                    jnp.where(first, cosw, pltpu.roll(sinw, HALF, 1)),
                    jnp.where(first, pltpu.roll(cosw, HALF, 1), sinw),
                ],
                axis=1,
            )
            high, low = split(pair)
            fold_high[g * size : (g + 1) * size] = high
            fold_low[g * size : (g + 1) * size] = low
        total = dot(tok_s[...], fold_high[...]) + dot(tok_s[...], fold_low[...])
        for core in range(2):
            target = goal * 2 + core
            block = total[:, core * LANES : (core + 1) * LANES]
            peak = jnp.max(jnp.abs(block), axis=1, keepdims=True)
            peak = jnp.max(peak, axis=0, keepdims=True)
            scale = jnp.broadcast_to(jnp.maximum(peak, 1e-30) * 1.0079, (EXTRA, LANES))
            scale = scale.astype(jnp.bfloat16)
            factor = CODE / scale[0:1].astype(jnp.float32)
            code = jnp.exp(jnp.abs(block) * factor) - 1.0
            code = jnp.where(block < 0.0, -code, code).astype(jnp.bfloat16)
            for part in range(PARTS):
                rows = slice(part * part_rows, (part + 1) * part_rows)
                send_a[part, target, :part_rows] = code[rows]
                send_a[part, target, part_rows:] = scale

        def ship(parts, steps):
            for part in parts:
                for at in steps:
                    for core in range(2):
                        copy_a(part, peer_at(at, chip) * 2 + core).start()

        half = range(PARTS // 2)
        rest = range(PARTS // 2, PARTS)

        @pl.when(step == 0)
        def _():
            pl.semaphore_wait(barrier, count - 1)
            ship(half, [0])

        @pl.when(step == 1)
        def _():
            ship(half, [1])
            ship(range(PARTS // 2, PARTS - 1), [0, 1])

        @pl.when(step == 2)
        def _():
            ship(half, [2])
            ship(range(PARTS // 2, PARTS - 1), [2])
            ship(range(PARTS - 1, PARTS), [0, 1, 2])

        @pl.when(step == chips - 1)
        def _():
            for part in range(PARTS):
                copy_a(part, chip * 2 + (1 - me % 2)).start()
                recv_a[part, me] = send_a[part, me]

    for pair in range(RADIX // 2):

        def take(at, base):
            source = base + at

            @pl.when(source != me)
            def _():
                pltpu.make_async_remote_copy(
                    src_ref=send_a.at[pair, source],
                    dst_ref=recv_a.at[pair, source],
                    send_sem=send_a_sem.at[pair, source],
                    recv_sem=recv_a_sem.at[pair, source],
                    device_id={"row": source},
                    device_id_type=pl.DeviceIdType.MESH,
                ).wait_recv()

            factor = recv_a[pair, source, part_rows:].astype(jnp.float32)[0:1]
            factor = factor * (scaling / CODE)
            code = recv_a[pair, source, :part_rows].astype(jnp.float32)
            value = jnp.log(1.0 + jnp.abs(code)) * factor
            value = jnp.where(code < 0.0, -value, value)
            high, low = split(value)
            rows = pl.ds(pl.multiple_of(source * inner, inner), inner)
            for half in range(2):
                span = slice((pair * 2 + half) * LANES, (pair * 2 + half + 1) * LANES)
                zhigh[rows, span] = high[half * inner : (half + 1) * inner]
                zlow[rows, span] = low[half * inner : (half + 1) * inner]

        def near_or_far(base):
            pl.loop(0, count // 2)(lambda at: take(at, base))
            span = pl.ds(pl.multiple_of(base * inner, size // 2), size // 2)
            terms = dot(high_ref[:, span], zhigh[span, cols])
            terms += dot(high_ref[:, span], zlow[span, cols])
            return terms + dot(low_ref[:, span], zhigh[span, cols])

        cols = slice(pair * 2 * LANES, (pair + 1) * 2 * LANES)
        own = (me // (count // 2)) * (count // 2)
        found_s[...] = near_or_far(own)
        found = found_s[...] + near_or_far(count // 2 - own)
        for half in range(2):
            t = pair * 2 + half
            cosz = found[:size, half * LANES : (half + 1) * LANES]
            sinz = found[size:, half * LANES : (half + 1) * LANES]
            whole = cosz + sign * pltpu.roll(sinz, HALF, 1)
            if t:
                whole = twist_ref[:, t : t + 1] * whole + (
                    twist_ref[:, RADIX + t : RADIX + t + 1] * sign
                ) * pltpu.roll(whole, HALF, 1)
            turned[t] = whole

    @pl.loop(0, count)
    def _(at):
        target = peer_at(at // 2, chip) * 2 + at % 2
        weights = last_ref[target]
        rows_at = 32
        for chunk in range(mid // rows_at):
            upper = slice(chunk * rows_at, (chunk + 1) * rows_at)
            under = slice(mid + chunk * rows_at, mid + (chunk + 1) * rows_at)
            top = weights[0:1] * turned[0, upper]
            bottom = weights[0:1] * turned[0, under]
            for t in range(1, RADIX):
                top += weights[t : t + 1] * turned[t, upper]
                bottom += weights[t : t + 1] * turned[t, under]
            packed = jnp.where(first, top, bottom) + pltpu.roll(
                jnp.where(first, bottom, top), HALF, 1
            )
            packed = packed.astype(jnp.bfloat16)
            send_b[target, upper] = packed

        @pl.when(target != me)
        def _():
            copy_b(target).start()

    recv_b[me] = send_b[me]

    for at in range(chips):
        goal = peer_at(chips - 1 - at, chip)
        for core in range(2):
            source = goal * 2 + core

            @pl.when(source != me)
            def _():
                pltpu.make_async_remote_copy(
                    src_ref=send_b.at[source],
                    dst_ref=recv_b.at[source],
                    send_sem=send_b_sem.at[source],
                    recv_sem=recv_b_sem.at[source],
                    device_id={"row": source},
                    device_id_type=pl.DeviceIdType.MESH,
                ).wait_recv()

        left = recv_b[goal * 2].astype(jnp.float32)
        right = recv_b[goal * 2 + 1].astype(jnp.float32)
        cols = pl.ds(pl.multiple_of(goal * LANES, LANES), LANES)
        out_ref[:mid, cols] = jnp.where(first, left, pltpu.roll(right, HALF, 1)).astype(
            jnp.bfloat16
        )
        out_ref[mid:, cols] = jnp.where(first, pltpu.roll(left, HALF, 1), right).astype(
            jnp.bfloat16
        )

    @pl.loop(1, count)
    def _(ahead):
        target = lax.rem(me + ahead, count)
        for part in range(PARTS):
            copy_a(part, target).wait_send()
        copy_b(target).wait_send()


def kernel_body(count, tokens, out_weight):
    size = tokens.shape[0]
    length = size * count
    scaling = 1.0 / math.sqrt(length * GROUP_DIM)
    vmem = pl.BlockSpec(memory_space=pltpu.VMEM)
    consts = [jnp.asarray(table) for table in tables(size, length)]
    return pl.pallas_call(
        functools.partial(kernel, scaling, count),
        out_shape=jax.ShapeDtypeStruct((size, out_weight.shape[1]), jnp.bfloat16),
        in_specs=[pl.BlockSpec(memory_space=pl.ANY)] * 4 + [vmem] * 2,
        out_specs=vmem,
        scratch_shapes=[
            pltpu.VMEM(tokens.shape, jnp.bfloat16),
            pltpu.VMEM(out_weight.shape, jnp.bfloat16),
            pltpu.VMEM((2 * size, size), jnp.bfloat16),
            pltpu.VMEM((2 * size, size), jnp.bfloat16),
            pltpu.VMEM(tokens.shape, jnp.bfloat16),
            pltpu.VMEM((PARTS, count, size // PARTS + EXTRA, LANES), jnp.bfloat16),
            pltpu.VMEM((PARTS, count, size // PARTS + EXTRA, LANES), jnp.bfloat16),
            pltpu.VMEM((size, RADIX * LANES), jnp.bfloat16),
            pltpu.VMEM((size, RADIX * LANES), jnp.bfloat16),
            pltpu.VMEM((RADIX, size, LANES), jnp.float32),
            pltpu.VMEM((2 * size, 2 * LANES), jnp.float32),
            pltpu.VMEM((tokens.shape[1], 2 * LANES), jnp.bfloat16),
            pltpu.VMEM((tokens.shape[1], 2 * LANES), jnp.bfloat16),
            pltpu.VMEM((count, size // 2, LANES), jnp.bfloat16),
            pltpu.VMEM((count, size // 2, LANES), jnp.bfloat16),
            pltpu.SemaphoreType.DMA((7,)),
            pltpu.SemaphoreType.DMA((PARTS, count)),
            pltpu.SemaphoreType.DMA((PARTS, count)),
            pltpu.SemaphoreType.DMA((count,)),
            pltpu.SemaphoreType.DMA((count,)),
        ],
        compiler_params=pltpu.CompilerParams(
            collective_id=0, has_side_effects=True, vmem_limit_bytes=60 * 1024 * 1024
        ),
    )(tokens, out_weight, *consts)


def body(tokens, out_weight):
    size = tokens.shape[0]
    count = lax.axis_size("row")
    fits = (
        count == RADIX
        and size == GROUP_DIM
        and tokens.shape[1] == GROUPS * GROUP_DIM
        and out_weight.shape[1] == count * HALF
    )
    if fits:
        return kernel_body(count, tokens, out_weight)
    return general_body(tokens, out_weight)


def solution(mesh):
    placed = (P("row", None), P(None, "col"))
    return jax.shard_map(
        body, mesh=mesh, in_specs=placed, out_specs=P("row", "col"), check_vma=False
    )
```

profile of v0, /device:TPU:1, one launch (start us, length us, event | category | flops | bytes accessed | tf_op | source)
XLA Modules:
  0.0 51.6 jit_solution(3222545057575129155)
XLA Ops:
  0.0 49.8 %shard_map.64 = bf16[512,512]{1,0:T(8,128)(2,1)} custom-call(bf16[512,2048]{1,0:T(8,128)(2,1)} %tok_hbm.1, bf16[2048,512]{1,0:T(8,128)(2,1)} %w_hbm.1, bf16[1024,512]{1,0:T(8,128)(2,1)} %constant.8.clone.high_hbm, bf16[1024,512]{1,0:T(8,128)(2,1)} %constant.9.clone.low_hbm, f32[512,128]{1,0:T(8,128)} %constant.10.clone.twist_ref, ...), custom_call_target="tpu_custom_call" | custom-call | tf_op jit(solution)/shard_map/pallas_call | solution.py:424
  49.8 1.9 %copy.8 = bf16[512,512]{1,0:T(8,128)(2,1)} copy(bf16[512,512]{1,0:T(8,128)(2,1)} %shard_map.64) | data formatting | bytes 1048576
where the time goes:
time: 52.5 us; the launch traced here: 51.6 us
  Pallas kernels  49.8 us (95%)
  local copies, waits for them, and re-layouts  1.87 us (4%)
    pallas_call x1, Pallas kernels, kernel_body(): pl.pallas_call(functools.partial(kernel, scaling, count), out_shape=jax.S...  49.8 us
    unnamed x1, local copies, waits for them, and re-layouts  1.87 us

commit v1 on v0

v1 whole, which is shorter than its diff:
```python
import math

import functools

import jax
import jax.numpy as jnp
import numpy as np
from jax import lax
from jax.experimental import pallas as pl
from jax.experimental.pallas import tpu as pltpu
from jax.sharding import PartitionSpec as P

GROUPS = 4
GROUP_DIM = 512


def angles(product, period):
    return (product % period).astype(jnp.float32) * (2.0 * math.pi / period)


def plain_dot(matrix, values):
    return jnp.dot(
        matrix, values, precision=lax.Precision.HIGHEST, preferred_element_type=jnp.float32
    )


def whole_transform(whole_rows, row_count, seg_rows, length):
    few_chans = whole_rows.shape[2]
    lattice = jnp.arange(row_count, dtype=jnp.int32)
    phases = angles(lattice[:, None] * lattice[None, :], row_count)
    cosine_table = jnp.cos(phases)
    sine_table = jnp.sin(phases)
    real_in = whole_rows[0].reshape(row_count, seg_rows * few_chans)
    imag_in = whole_rows[1].reshape(row_count, seg_rows * few_chans)
    first_re = (plain_dot(cosine_table, real_in) + plain_dot(sine_table, imag_in)).reshape(
        row_count, seg_rows, few_chans
    )
    first_im = (plain_dot(cosine_table, imag_in) - plain_dot(sine_table, real_in)).reshape(
        row_count, seg_rows, few_chans
    )
    inner = jnp.arange(seg_rows, dtype=jnp.int32)
    twist = angles(lattice[:, None] * inner[None, :], length)[:, :, None]
    twist_cos = jnp.cos(twist)
    twist_sin = jnp.sin(twist)
    turned_re = twist_cos * first_re + twist_sin * first_im
    turned_im = twist_cos * first_im - twist_sin * first_re
    folded_re = jnp.transpose(turned_re, (1, 0, 2)).reshape(seg_rows, row_count * few_chans)
    folded_im = jnp.transpose(turned_im, (1, 0, 2)).reshape(seg_rows, row_count * few_chans)
    seg_phases = angles(inner[:, None] * inner[None, :], seg_rows)
    real_part = plain_dot(jnp.cos(seg_phases), folded_re) + plain_dot(
        jnp.sin(seg_phases), folded_im
    )
    return real_part.reshape(length, few_chans)


def general_body(tokens, out_weight):
    seg_rows = tokens.shape[0]
    col_width = out_weight.shape[1]
    row_count = lax.axis_size("row")
    length = seg_rows * row_count
    scaling = 1.0 / math.sqrt(length * GROUP_DIM)
    weight_wide = out_weight.astype(jnp.float32)
    lattice = jnp.arange(GROUP_DIM, dtype=jnp.int32)
    phases = angles(lattice[:, None] * lattice[None, :], GROUP_DIM)
    cosine_table = jnp.cos(phases) * scaling
    sine_table = jnp.sin(phases) * scaling
    folded_rows = []
    for group in range(GROUPS):
        group_rows = weight_wide[group * GROUP_DIM : (group + 1) * GROUP_DIM]
        folded_rows.append(
            jnp.concatenate(
                [plain_dot(cosine_table, group_rows), -plain_dot(sine_table, group_rows)], axis=1
            )
        )
    folded_map = jnp.concatenate(folded_rows, axis=0)
    spectrum = plain_dot(tokens.astype(jnp.float32), folded_map)
    stacked = jnp.stack([spectrum[:, :col_width], spectrum[:, col_width:]])
    whole_rows = lax.all_to_all(stacked, "row", split_axis=2, concat_axis=1, tiled=True)
    ordered = whole_transform(whole_rows, row_count, seg_rows, length)
    spectral = lax.all_to_all(
        ordered.astype(jnp.bfloat16), "row", split_axis=0, concat_axis=1, tiled=True
    )
    return spectral

RADIX = 8
HALF = 64
QUARTER = 32
LANES = 128
EXTRA = 16
ROWS = 8
COLS = 4
SLOTS = 8
CODE = 84.0
LATE = 4
TALL = 32
UNROLL = 2
MESH = pl.DeviceIdType.MESH


def split_table(values):
    big = values.astype(jnp.bfloat16)
    return big, (values - big.astype(np.float64)).astype(jnp.bfloat16)


def tables(size, length):
    index = np.arange(size)
    phase = 2.0 * np.pi * ((index[:, None] * index[None, :]) % size) / size
    high, low = split_table(np.concatenate([np.cos(phase), np.sin(phase)], axis=0))
    turn = 2.0 * np.pi * (index[:, None] * np.arange(RADIX)[None, :]) / length
    twist = np.zeros((size, LANES), np.float32)
    twist[:, :RADIX] = np.cos(turn)
    twist[:, RADIX : 2 * RADIX] = np.sin(turn)
    return high, low, twist


def dot(a, b):
    return jnp.dot(a, b, preferred_element_type=jnp.float32)


def split(values):
    high = values.astype(jnp.bfloat16)
    return high, (values - high.astype(jnp.float32)).astype(jnp.bfloat16)


def row_of(slot, upper):
    return ROWS // 4 + upper * (ROWS // 4) + slot % 2


def kernel(
    scaling,
    tok_hbm,
    w_hbm,
    high_hbm,
    low_hbm,
    twist_ref,
    out_ref,
    tok_ref,
    w_ref,
    high_ref,
    low_ref,
    tok_s,
    tok_r,
    turn_c,
    turn_s,
    found,
    packed,
    code_s,
    gathered,
    fold_high,
    fold_low,
    total,
    load_sem,
    tok_send,
    tok_recv,
    code_send,
    code_recv,
    side_send,
    side_recv,
):
    me = lax.axis_index("row")
    col = lax.axis_index("col")
    size = tok_ref.shape[0]
    inner = size // RADIX
    mid = size // 2
    groups = w_ref.shape[0] // size
    upper = me // (ROWS // 2)
    central = jnp.logical_and(me >= ROWS // 4, me < 3 * ROWS // 4)
    core = me % 2
    beside = col + 1 - 2 * (col % 2)
    across = col + 2 - 4 * (col // 2)
    corner = COLS - 1 - col

    cols = pl.ds(pl.multiple_of(col * size, size), size)
    load_tok = pltpu.make_async_copy(tok_hbm.at[:, cols], tok_ref, load_sem.at[0])
    load_high = pltpu.make_async_copy(high_hbm, high_ref, load_sem.at[1])
    load_low = pltpu.make_async_copy(low_hbm, low_ref, load_sem.at[2])
    load_w = pltpu.make_async_copy(w_hbm, w_ref, load_sem.at[3])
    for load in (load_tok, load_w, load_high, load_low):
        load.start()
    barrier = pltpu.get_barrier_semaphore()
    for ahead in range(1, ROWS):
        pl.semaphore_signal(
            barrier, inc=1, device_id={"row": lax.rem(me + ahead, ROWS)}, device_id_type=MESH
        )
    for other in (beside, across, corner):
        pl.semaphore_signal(barrier, inc=1, device_id={"col": other}, device_id_type=MESH)

    lane = lax.broadcasted_iota(jnp.int32, (1, LANES), 1)
    first = lane < HALF
    cosine_lane = (lane % HALF) < QUARTER

    spot = lax.broadcasted_iota(jnp.int32, (1, size), 1)
    which = spot % HALF
    pair = (spot // HALF) * QUARTER + which % QUARTER
    partner = jnp.where(pair == 0, mid, size - pair)
    wanted = jnp.where(which < QUARTER, pair, partner)
    place = lax.broadcasted_iota(jnp.int32, (size, size), 0)
    pick = jnp.where(place == wanted, 1.0, 0.0).astype(jnp.bfloat16)
    down = lax.broadcasted_iota(jnp.int32, (size, 1), 0)
    residue = 2 * ((down % mid) // inner) + down // mid
    source = RADIX * (down % inner) + residue
    along = lax.broadcasted_iota(jnp.int32, (size, size), 1)
    order = jnp.where(along == source, 1.0, 0.0).astype(jnp.bfloat16)
    load_tok.wait()
    chosen = dot(tok_ref[...], pick).astype(jnp.bfloat16)
    ordered = dot(order, chosen)
    for tile in range(COLS):
        span = slice(tile * LANES, (tile + 1) * LANES)
        even = ordered[:mid, span]
        odd = ordered[mid:, span]
        left = jnp.where(first, even, pltpu.roll(odd, HALF, 1)).astype(jnp.bfloat16)
        right = jnp.where(first, pltpu.roll(even, HALF, 1), odd).astype(jnp.bfloat16)
        for v in range(4):
            tok_s[2 * tile, v] = left[v * inner : (v + 1) * inner]
            tok_s[2 * tile + 1, v] = right[v * inner : (v + 1) * inner]

    def token_copy(at, far, target):
        turn = at // 2
        return pltpu.make_async_remote_copy(
            src_ref=tok_s.at[at],
            dst_ref=tok_r.at[turn, :, pl.ds(pl.multiple_of(me * inner, inner), inner), :],
            send_sem=tok_send.at[at, far],
            recv_sem=tok_recv.at[turn, me],
            device_id={"row": target},
            device_id_type=MESH,
        )

    pl.semaphore_wait(barrier, ROWS - 1 + COLS - 1)

    @pl.loop(0, SLOTS)
    def _(at):
        token_copy(at, 1, row_of(at, 1 - upper)).start()
        near = row_of(at, upper)

        @pl.when(near != me)
        def _():
            token_copy(at, 0, near).start()

        @pl.when(near == me)
        def _():
            rows = pl.ds(pl.multiple_of(me * inner, inner), inner)
            for v in range(4):
                tok_r[at // 2, v, rows, :] = tok_s[at, v]

    for v in range(4):
        for start in range(0, size, LANES):
            rows = slice(start, start + LANES)
            turn_c[v, rows] = jnp.where(
                first, twist_ref[rows, 2 * v : 2 * v + 1], twist_ref[rows, 2 * v + 1 : 2 * v + 2]
            )
            turn_s[v, rows] = jnp.where(
                first,
                twist_ref[rows, RADIX + 2 * v : RADIX + 2 * v + 1],
                twist_ref[rows, RADIX + 2 * v + 1 : RADIX + 2 * v + 2],
            )

    load_high.wait()
    load_low.wait()
    load_w.wait()
    parity = lax.broadcasted_iota(jnp.int32, (EXTRA, size), 1) % 2
    swing = (1 - 2 * parity).astype(jnp.float32).astype(jnp.bfloat16)

    @pl.loop(0, groups)
    def _(g):
        side = w_ref[pl.ds(pl.multiple_of(g * size, size), size), :]
        wave = dot(high_ref[:mid], side) + dot(low_ref[:mid], side)
        sine = dot(high_ref[size : size + mid], side) + dot(low_ref[size : size + mid], side)
        last = dot(swing, side)[0:1]
        begin = pl.multiple_of(g * HALF, HALF)
        for slot in range(SLOTS):
            rows = slice(slot * QUARTER, (slot + 1) * QUARTER)
            high, low = split(wave[rows])
            fold_high[slot, pl.ds(begin, QUARTER), :] = high
            fold_low[slot, pl.ds(begin, QUARTER), :] = low
            block = -sine[rows]
            if slot == 0:
                top = lax.broadcasted_iota(jnp.int32, block.shape, 0) == 0
                block = jnp.where(top, last, block)
            high, low = split(block)
            begin_odd = pl.multiple_of(g * HALF + QUARTER, QUARTER)
            fold_high[slot, pl.ds(begin_odd, QUARTER), :] = high
            fold_low[slot, pl.ds(begin_odd, QUARTER), :] = low

    total[...] = jnp.zeros_like(total)

    def code_copy(at, quarter):
        return pltpu.make_async_remote_copy(
            src_ref=code_s.at[at // 2, quarter],
            dst_ref=gathered.at[at, col],
            send_sem=code_send.at[at // 2, quarter],
            recv_sem=code_recv.at[at],
            device_id={"row": upper * 4 + quarter},
            device_id_type=MESH,
        )

    def side_copy(at, origin, target, which):
        return pltpu.make_async_remote_copy(
            src_ref=gathered.at[at, origin],
            dst_ref=gathered.at[at, origin],
            send_sem=side_send.at[at, which],
            recv_sem=side_recv.at[at, origin],
            device_id={"col": target},
            device_id_type=MESH,
        )

    def part(turn, base):
        @pl.loop(base * 4, base * 4 + 4)
        def _(source):
            @pl.when(source != me)
            def _():
                rows = pl.ds(pl.multiple_of(source * inner, inner), inner)
                pltpu.make_async_remote_copy(
                    src_ref=tok_s.at[0],
                    dst_ref=tok_r.at[turn, :, rows, :],
                    send_sem=tok_send.at[0, 0],
                    recv_sem=tok_recv.at[turn, source],
                    device_id={"row": source},
                    device_id_type=MESH,
                ).wait_recv()

        span = pl.ds(pl.multiple_of(base * mid, mid), mid)
        terms = []
        for v in range(0, 4, 2):
            both = jnp.concatenate([tok_r[turn, v, span, :], tok_r[turn, v + 1, span, :]], axis=1)
            terms.append(dot(high_ref[:, span], both) + dot(low_ref[:, span], both))
        return terms

    def prepare(at):
        for v, term in enumerate(part(at // 2, upper)):
            found[:, 2 * v * LANES : 2 * (v + 1) * LANES] = term

    def spread(at):
        for which, target in enumerate((beside, across, corner)):
            side_copy(at, col, target, which).start()

    def produce(at):
        turn = at // 2
        for v, term in enumerate(part(turn, 1 - upper)):
            found[:, 2 * v * LANES : 2 * (v + 1) * LANES] += term

        sign = (1 - 2 * upper).astype(jnp.float32)
        lone = jnp.logical_and(lane % QUARTER == 0, at == 0)
        straight = jnp.logical_or(cosine_lane, lone)
        weights = []
        for q in range(4):
            angle = math.pi * q / 4
            weights.append(
                (
                    jnp.where(first, 1.0, sign * math.cos(angle)),
                    jnp.where(first, 0.0, sign * math.sin(angle)),
                )
            )
        tall = TALL

        def rows_of(begin):
            rows = pl.ds(begin, tall)
            lower = pl.ds(begin + size, tall)
            re, im = [], []
            for v in range(4):
                span = slice(v * LANES, (v + 1) * LANES)
                a, b = found[rows, span], found[lower, span]
                c, s = turn_c[v, rows], turn_s[v, rows]
                re.append(c * a - s * b)
                im.append(s * a + c * b)
            pr, pi = re[0] + re[2], im[0] + im[2]
            mr, mi = re[0] - re[2], im[0] - im[2]
            sr, si = re[1] + re[3], im[1] + im[3]
            dr, di = re[1] - re[3], im[1] - im[3]
            fours = [
                (pr + sr, pi + si),
                (mr - di, mi + dr),
                (pr - sr, pi - si),
                (mr + di, mi - dr),
            ]
            results = []
            for (a, b), (c, s) in zip(fours, weights):
                xr = c * a - s * b
                xi = s * a + c * b
                keep = jnp.where(straight, xr, -xi)
                move = jnp.where(lone, 0.0, jnp.where(cosine_lane, xi, xr))
                results.append(keep + pltpu.roll(move, QUARTER, 1))
            return results

        def chunk(step, peak):
            begin = pl.multiple_of(step * tall, tall)
            ones = rows_of(begin)
            twos = rows_of(pl.multiple_of(begin + mid, tall))
            for q in range(4):
                value = jnp.where(first, ones[q], twos[q]) + pltpu.roll(
                    jnp.where(first, twos[q], ones[q]), HALF, 1
                )
                packed[q, pl.ds(begin, tall), :] = value
                peak = jnp.maximum(peak, jnp.abs(value))
            return peak

        peak = jnp.zeros((tall, LANES), jnp.float32)
        peak = lax.fori_loop(0, mid // tall, chunk, peak, unroll=UNROLL)
        peak = jnp.max(peak, axis=0, keepdims=True)
        scale = jnp.broadcast_to(jnp.maximum(peak, 1e-30) * 1.0079, (EXTRA, LANES))
        scale = scale.astype(jnp.bfloat16)
        factor = CODE / scale[0:1].astype(jnp.float32)

        @pl.loop(0, 4)
        def _(q):
            block = packed[q]
            code = jnp.exp(jnp.abs(block) * factor) - 1.0
            code = jnp.where(block < 0.0, -code, code).astype(jnp.bfloat16)
            mine = upper * 4 + q == me

            @pl.when(mine)
            def _():
                gathered[at, col, :mid] = code
                gathered[at, col, mid:] = scale
                spread(at)

            @pl.when(jnp.logical_not(mine))
            def _():
                code_s[turn, q, :mid] = code
                code_s[turn, q, mid:] = scale
                code_copy(at, q).start()

    def forward(at):
        pltpu.make_async_remote_copy(
            src_ref=code_s.at[0, 0],
            dst_ref=gathered.at[at, col],
            send_sem=code_send.at[0, 0],
            recv_sem=code_recv.at[at],
            device_id={"row": row_of(at, upper)},
            device_id_type=MESH,
        ).wait_recv()
        spread(at)

    def contract(at):
        for origin in (beside, across, corner):
            side_copy(at, origin, origin, 0).wait_recv()
        tops, bottoms = [], []
        for pair_at in range(2):
            values = []
            for c in (2 * pair_at, 2 * pair_at + 1):
                factor = gathered[at, c, mid:].astype(jnp.float32)[0:1] * (scaling / CODE)
                code = gathered[at, c, :mid].astype(jnp.float32)
                value = jnp.log(1.0 + jnp.abs(code)) * factor
                values.append(jnp.where(code < 0.0, -value, value))
            tops.append(jnp.where(first, values[0], pltpu.roll(values[1], HALF, 1)))
            bottoms.append(jnp.where(first, pltpu.roll(values[0], HALF, 1), values[1]))
        for half, parts in enumerate((tops, bottoms)):
            rows = slice(half * mid, (half + 1) * mid)
            high, low = split(jnp.concatenate(parts, axis=1))
            terms = dot(high, fold_high[at]) + dot(low, fold_high[at])
            total[rows] += terms + dot(high, fold_low[at])

    def owns(at):
        return jnp.logical_and(at < SLOTS, jnp.logical_and(central, core == at % 2))

    @pl.when(owns(0))
    def _():
        prepare(0)

    @pl.loop(0, SLOTS + LATE)
    def _(step):
        @pl.when(owns(step))
        def _():
            produce(step)

        @pl.when(jnp.logical_and(step >= 1, step < SLOTS + 1))
        def _():
            @pl.when(jnp.logical_not(owns(step - 1)))
            def _():
                forward(step - 1)

        @pl.when(step >= LATE)
        def _():
            contract(step - LATE)

        @pl.when(owns(step + 1))
        def _():
            prepare(step + 1)

    out_ref[...] = total[...].astype(jnp.bfloat16)

    @pl.loop(0, SLOTS)
    def _(at):
        near = row_of(at, upper)
        token_copy(at, 1, row_of(at, 1 - upper)).wait_send()

        @pl.when(near != me)
        def _():
            token_copy(at, 0, near).wait_send()

        for which, target in enumerate((beside, across, corner)):
            side_copy(at, col, target, which).wait_send()

        @pl.when(owns(at))
        def _():
            @pl.loop(0, 4)
            def _(q):
                @pl.when(upper * 4 + q != me)
                def _():
                    code_copy(at, q).wait_send()


def kernel_body(tokens, out_weight):
    size = tokens.shape[0]
    length = size * ROWS
    scaling = 1.0 / math.sqrt(length * GROUP_DIM)
    vmem = pl.BlockSpec(memory_space=pltpu.VMEM)
    consts = [jnp.asarray(table) for table in tables(size, length)]
    bf16, f32 = jnp.bfloat16, jnp.float32
    dma = pltpu.SemaphoreType.DMA
    return pl.pallas_call(
        functools.partial(kernel, scaling),
        out_shape=jax.ShapeDtypeStruct((size, out_weight.shape[1]), bf16),
        in_specs=[pl.BlockSpec(memory_space=pl.ANY)] * 4 + [vmem],
        out_specs=vmem,
        scratch_shapes=[
            pltpu.VMEM((size, size), bf16),
            pltpu.VMEM(out_weight.shape, bf16),
            pltpu.VMEM((2 * size, size), bf16),
            pltpu.VMEM((2 * size, size), bf16),
            pltpu.VMEM((SLOTS, 4, size // RADIX, LANES), bf16),
            pltpu.VMEM((4, 4, size, LANES), bf16),
            pltpu.VMEM((4, size, LANES), f32),
            pltpu.VMEM((4, size, LANES), f32),
            pltpu.VMEM((2 * size, 4 * LANES), f32),
            pltpu.VMEM((4, size // 2, LANES), f32),
            pltpu.VMEM((4, 4, size // 2 + EXTRA, LANES), bf16),
            pltpu.VMEM((SLOTS, COLS, size // 2 + EXTRA, LANES), bf16),
            pltpu.VMEM((SLOTS, COLS * HALF, out_weight.shape[1]), bf16),
            pltpu.VMEM((SLOTS, COLS * HALF, out_weight.shape[1]), bf16),
            pltpu.VMEM((size, out_weight.shape[1]), f32),
            dma((4,)),
            dma((SLOTS, 2)),
            dma((4, ROWS)),
            dma((4, 4)),
            dma((SLOTS,)),
            dma((SLOTS, 3)),
            dma((SLOTS, COLS)),
        ],
        compiler_params=pltpu.CompilerParams(
            collective_id=0, has_side_effects=True, vmem_limit_bytes=60 * 1024 * 1024
        ),
    )(tokens, out_weight, *consts)


def body(tokens, out_weight):
    size = tokens.shape[0]
    fits = (
        lax.axis_size("row") == ROWS
        and lax.axis_size("col") == COLS
        and size == GROUP_DIM
        and tokens.shape[1] == COLS * GROUP_DIM
        and out_weight.shape[1] == GROUP_DIM
    )
    if fits:
        return kernel_body(tokens, out_weight)
    return general_body(tokens, out_weight)


def solution(mesh):
    placed = (P("row", None), P(None, "col"))
    return jax.shard_map(
        body, mesh=mesh, in_specs=placed, out_specs=P("row", "col"), check_vma=False
    )
```

time: 52.5 us -> 50.5 us (0.962)
  Pallas kernels: 49.8 us -> 47.9 us
    pallas_call x1, Pallas kernels: 49.8 us -> 47.9 us  [kernel_body(): pl.pallas_call(functools.partial(kernel, scaling), out_shape=jax.ShapeDty...]
where the time goes in v1:
time: 50.5 us; the launch traced here: 49.8 us
  Pallas kernels  47.9 us (95%)
  local copies, waits for them, and re-layouts  1.87 us (4%)
    pallas_call x1, Pallas kernels, kernel_body(): pl.pallas_call(functools.partial(kernel, scaling), out_shape=jax.ShapeDty...  47.9 us
    unnamed x1, local copies, waits for them, and re-layouts  1.87 us

profile of v1, /device:TPU:1, one launch (start us, length us, event | category | flops | bytes accessed | tf_op | source)
XLA Modules:
  0.0 49.8 jit_solution(4009852399905499871)
XLA Ops:
  0.0 47.9 %shard_map.55 = bf16[512,512]{1,0:T(8,128)(2,1)} custom-call(bf16[512,2048]{1,0:T(8,128)(2,1)} %tok_hbm.1, bf16[2048,512]{1,0:T(8,128)(2,1)} %w_hbm.1, bf16[1024,512]{1,0:T(8,128)(2,1)} %constant.6.clone.high_hbm, bf16[1024,512]{1,0:T(8,128)(2,1)} %constant.7.clone.low_hbm, f32[512,128]{1,0:T(8,128)} %constant.8.clone.twist_ref), custom_call_target="tpu_custom_call" | custom-call | tf_op jit(solution)/shard_map/pallas_call | solution.py:510
  47.9 1.9 %copy.7 = bf16[512,512]{1,0:T(8,128)(2,1)} copy(bf16[512,512]{1,0:T(8,128)(2,1)} %shard_map.55) | data formatting | bytes 1048576

commit v2 on v1

--- a/solution.py
+++ b/solution.py
@@ -91,9 +91,12 @@
 COLS = 4
 SLOTS = 8
 CODE = 84.0
-LATE = 4
+LATE = 5
+LATER = 3
+INNER = 6
+OUTER = 6
 TALL = 32
-UNROLL = 2
+UNROLL = 4
 MESH = pl.DeviceIdType.MESH
 
 
@@ -132,12 +135,13 @@
     w_hbm,
     high_hbm,
     low_hbm,
-    twist_ref,
+    twist_hbm,
     out_ref,
     tok_ref,
     w_ref,
     high_ref,
     low_ref,
+    twist_ref,
     tok_s,
     tok_r,
     turn_c,
@@ -162,7 +166,7 @@
     size = tok_ref.shape[0]
     inner = size // RADIX
     mid = size // 2
-    groups = w_ref.shape[0] // size
+    groups = COLS
     upper = me // (ROWS // 2)
     central = jnp.logical_and(me >= ROWS // 4, me < 3 * ROWS // 4)
     core = me % 2
@@ -175,8 +179,8 @@
     load_high = pltpu.make_async_copy(high_hbm, high_ref, load_sem.at[1])
     load_low = pltpu.make_async_copy(low_hbm, low_ref, load_sem.at[2])
     load_w = pltpu.make_async_copy(w_hbm, w_ref, load_sem.at[3])
-    for load in (load_tok, load_w, load_high, load_low):
-        load.start()
+    load_twist = pltpu.make_async_copy(twist_hbm, twist_ref, load_sem.at[4])
+    load_tok.start()
     barrier = pltpu.get_barrier_semaphore()
     for ahead in range(1, ROWS):
         pl.semaphore_signal(
@@ -184,6 +188,9 @@
         )
     for other in (beside, across, corner):
         pl.semaphore_signal(barrier, inc=1, device_id={"col": other}, device_id_type=MESH)
+
+    for load in (load_twist, load_high, load_low, load_w):
+        load.start()
 
     lane = lax.broadcasted_iota(jnp.int32, (1, LANES), 1)
     first = lane < HALF
@@ -201,19 +208,6 @@
     source = RADIX * (down % inner) + residue
     along = lax.broadcasted_iota(jnp.int32, (size, size), 1)
     order = jnp.where(along == source, 1.0, 0.0).astype(jnp.bfloat16)
-    load_tok.wait()
-    chosen = dot(tok_ref[...], pick).astype(jnp.bfloat16)
-    ordered = dot(order, chosen)
-    for tile in range(COLS):
-        span = slice(tile * LANES, (tile + 1) * LANES)
-        even = ordered[:mid, span]
-        odd = ordered[mid:, span]
-        left = jnp.where(first, even, pltpu.roll(odd, HALF, 1)).astype(jnp.bfloat16)
-        right = jnp.where(first, pltpu.roll(even, HALF, 1), odd).astype(jnp.bfloat16)
-        for v in range(4):
-            tok_s[2 * tile, v] = left[v * inner : (v + 1) * inner]
-            tok_s[2 * tile + 1, v] = right[v * inner : (v + 1) * inner]
-
     def token_copy(at, far, target):
         turn = at // 2
         return pltpu.make_async_remote_copy(
@@ -225,23 +219,38 @@
             device_id_type=MESH,
         )
 
-    pl.semaphore_wait(barrier, ROWS - 1 + COLS - 1)
-
-    @pl.loop(0, SLOTS)
-    def _(at):
-        token_copy(at, 1, row_of(at, 1 - upper)).start()
-        near = row_of(at, upper)
-
-        @pl.when(near != me)
-        def _():
-            token_copy(at, 0, near).start()
-
-        @pl.when(near == me)
-        def _():
-            rows = pl.ds(pl.multiple_of(me * inner, inner), inner)
-            for v in range(4):
-                tok_r[at // 2, v, rows, :] = tok_s[at, v]
-
+    load_tok.wait()
+    for tile in range(COLS):
+        span = slice(tile * LANES, (tile + 1) * LANES)
+        chosen = dot(tok_ref[...], pick[:, span]).astype(jnp.bfloat16)
+        ordered = dot(order, chosen)
+        even = ordered[:mid]
+        odd = ordered[mid:]
+        left = jnp.where(first, even, pltpu.roll(odd, HALF, 1)).astype(jnp.bfloat16)
+        right = jnp.where(first, pltpu.roll(even, HALF, 1), odd).astype(jnp.bfloat16)
+        for v in range(4):
+            tok_s[2 * tile, v] = left[v * inner : (v + 1) * inner]
+            tok_s[2 * tile + 1, v] = right[v * inner : (v + 1) * inner]
+        if tile == 0:
+            pl.semaphore_wait(barrier, ROWS - 1 + COLS - 1)
+
+        @pl.loop(2 * tile, 2 * tile + 2)
+        def _(at):
+            near = row_of(at, upper)
+
+            @pl.when(near != me)
+            def _():
+                token_copy(at, 0, near).start()
+
+            token_copy(at, 1, row_of(at, 1 - upper)).start()
+
+            @pl.when(near == me)
+            def _():
+                rows = pl.ds(pl.multiple_of(me * inner, inner), inner)
+                for v in range(4):
+                    tok_r[at // 2, v, rows, :] = tok_s[at, v]
+
+    load_twist.wait()
     for v in range(4):
         for start in range(0, size, LANES):
             rows = slice(start, start + LANES)
@@ -254,14 +263,10 @@
                 twist_ref[rows, RADIX + 2 * v + 1 : RADIX + 2 * v + 2],
             )
 
-    load_high.wait()
-    load_low.wait()
-    load_w.wait()
     parity = lax.broadcasted_iota(jnp.int32, (EXTRA, size), 1) % 2
     swing = (1 - 2 * parity).astype(jnp.float32).astype(jnp.bfloat16)
 
-    @pl.loop(0, groups)
-    def _(g):
+    def fold(g):
         side = w_ref[pl.ds(pl.multiple_of(g * size, size), size), :]
         wave = dot(high_ref[:mid], side) + dot(low_ref[:mid], side)
         sine = dot(high_ref[size : size + mid], side) + dot(low_ref[size : size + mid], side)
@@ -329,15 +334,29 @@
         for v, term in enumerate(part(at // 2, upper)):
             found[:, 2 * v * LANES : 2 * (v + 1) * LANES] = term
 
+    relayed = jnp.where(central, INNER, OUTER)
+
     def spread(at):
-        for which, target in enumerate((beside, across, corner)):
-            side_copy(at, col, target, which).start()
+        side_copy(at, col, beside, 0).start()
+        side_copy(at, col, across, 1).start()
+
+        @pl.when(at >= relayed)
+        def _():
+            side_copy(at, col, corner, 2).start()
+
+    via = beside + core * (across - beside)
+    onward = across + core * (beside - across)
+
+    def relay(at):
+        side_copy(at, via, via, 2).wait_recv()
+        side_copy(at, via, onward, 2).start()
+
+    def finish(at):
+        for v, term in enumerate(part(at // 2, 1 - upper)):
+            found[:, 2 * v * LANES : 2 * (v + 1) * LANES] += term
 
     def produce(at):
         turn = at // 2
-        for v, term in enumerate(part(turn, 1 - upper)):
-            found[:, 2 * v * LANES : 2 * (v + 1) * LANES] += term
-
         sign = (1 - 2 * upper).astype(jnp.float32)
         lone = jnp.logical_and(lane % QUARTER == 0, at == 0)
         straight = jnp.logical_or(cosine_lane, lone)
@@ -401,7 +420,8 @@
         factor = CODE / scale[0:1].astype(jnp.float32)
 
         @pl.loop(0, 4)
-        def _(q):
+        def _(turn_at):
+            q = lax.rem(turn_at + 2 * upper, 4)
             block = packed[q]
             code = jnp.exp(jnp.abs(block) * factor) - 1.0
             code = jnp.where(block < 0.0, -code, code).astype(jnp.bfloat16)
@@ -431,8 +451,13 @@
         spread(at)
 
     def contract(at):
-        for origin in (beside, across, corner):
+        for origin in (onward, corner):
             side_copy(at, origin, origin, 0).wait_recv()
+
+        @pl.when(at >= relayed)
+        def _():
+            side_copy(at, via, via, 0).wait_recv()
+
         tops, bottoms = [], []
         for pair_at in range(2):
             values = []
@@ -452,6 +477,10 @@
     def owns(at):
         return jnp.logical_and(at < SLOTS, jnp.logical_and(central, core == at % 2))
 
+    load_high.wait()
+    load_low.wait()
+    load_w.wait()
+
     @pl.when(owns(0))
     def _():
         prepare(0)
@@ -460,7 +489,11 @@
     def _(step):
         @pl.when(owns(step))
         def _():
-            produce(step)
+            finish(step)
+
+        @pl.when(jnp.logical_and(step >= LATER, step < relayed + LATER))
+        def _():
+            relay(step - LATER)
 
         @pl.when(jnp.logical_and(step >= 1, step < SLOTS + 1))
         def _():
@@ -468,9 +501,17 @@
             def _():
                 forward(step - 1)
 
+        @pl.when(owns(step))
+        def _():
+            produce(step)
+
         @pl.when(step >= LATE)
         def _():
             contract(step - LATE)
+
+        @pl.when(step < groups)
+        def _():
+            fold(step)
 
         @pl.when(owns(step + 1))
         def _():
@@ -510,13 +551,14 @@
     return pl.pallas_call(
         functools.partial(kernel, scaling),
         out_shape=jax.ShapeDtypeStruct((size, out_weight.shape[1]), bf16),
-        in_specs=[pl.BlockSpec(memory_space=pl.ANY)] * 4 + [vmem],
+        in_specs=[pl.BlockSpec(memory_space=pl.ANY)] * 5,
         out_specs=vmem,
         scratch_shapes=[
             pltpu.VMEM((size, size), bf16),
             pltpu.VMEM(out_weight.shape, bf16),
             pltpu.VMEM((2 * size, size), bf16),
             pltpu.VMEM((2 * size, size), bf16),
+            pltpu.VMEM((size, LANES), f32),
             pltpu.VMEM((SLOTS, 4, size // RADIX, LANES), bf16),
             pltpu.VMEM((4, 4, size, LANES), bf16),
             pltpu.VMEM((4, size, LANES), f32),
@@ -528,7 +570,7 @@
             pltpu.VMEM((SLOTS, COLS * HALF, out_weight.shape[1]), bf16),
             pltpu.VMEM((SLOTS, COLS * HALF, out_weight.shape[1]), bf16),
             pltpu.VMEM((size, out_weight.shape[1]), f32),
-            dma((4,)),
+            dma((5,)),
             dma((SLOTS, 2)),
             dma((4, ROWS)),
             dma((4, 4)),

time: 50.5 us -> 48 us (0.950)
  Pallas kernels: 47.9 us -> 45.9 us
    pallas_call x1, Pallas kernels: 47.9 us -> 45.9 us  [kernel_body(): pl.pallas_call(functools.partial(kernel, scaling), out_shape=jax.ShapeDty...]
where the time goes in v2:
time: 48 us; the launch traced here: 47.8 us
  Pallas kernels  45.9 us (96%)
  local copies, waits for them, and re-layouts  1.87 us (4%)
    pallas_call x1, Pallas kernels, kernel_body(): pl.pallas_call(functools.partial(kernel, scaling), out_shape=jax.ShapeDty...  45.9 us
    unnamed x1, local copies, waits for them, and re-layouts  1.87 us

profile of v2, /device:TPU:1, one launch (start us, length us, event | category | flops | bytes accessed | tf_op | source)
XLA Modules:
  0.0 47.8 jit_solution(16641768617692942650)
XLA Ops:
  0.0 45.9 %shard_map.55 = bf16[512,512]{1,0:T(8,128)(2,1)} custom-call(bf16[512,2048]{1,0:T(8,128)(2,1)} %tok_hbm.1, bf16[2048,512]{1,0:T(8,128)(2,1)} %w_hbm.1, bf16[1024,512]{1,0:T(8,128)(2,1)} %constant.6.clone.high_hbm, bf16[1024,512]{1,0:T(8,128)(2,1)} %constant.7.clone.low_hbm, f32[512,128]{1,0:T(8,128)} %constant.8.clone.twist_hbm), custom_call_target="tpu_custom_call" | custom-call | tf_op jit(solution)/shard_map/pallas_call | solution.py:551
  45.9 1.9 %copy.7 = bf16[512,512]{1,0:T(8,128)(2,1)} copy(bf16[512,512]{1,0:T(8,128)(2,1)} %shard_map.55) | data formatting | bytes 1048576

commit v3 on v2

--- a/solution.py
+++ b/solution.py
@@ -93,7 +93,7 @@
 CODE = 84.0
 LATE = 5
 LATER = 3
-INNER = 6
+INNER = 7
 OUTER = 6
 TALL = 32
 UNROLL = 4
@@ -550,7 +550,7 @@
     dma = pltpu.SemaphoreType.DMA
     return pl.pallas_call(
         functools.partial(kernel, scaling),
-        out_shape=jax.ShapeDtypeStruct((size, out_weight.shape[1]), bf16),
+        out_shape=pltpu.VMEM((size, out_weight.shape[1]), bf16),
         in_specs=[pl.BlockSpec(memory_space=pl.ANY)] * 5,
         out_specs=vmem,
         scratch_shapes=[

time: 48 us -> 46.1 us (0.960)
  local copies, waits for them, and re-layouts: 1.87 us -> 0.8 us
  Pallas kernels: 45.9 us -> 45.1 us
    unnamed x1, local copies, waits for them, and re-layouts: 1.87 us -> 0.8 us
    pallas_call x1, Pallas kernels: 45.9 us -> 45.1 us  [kernel_body(): pl.pallas_call(functools.partial(kernel, scaling), out_shape=pltpu.VMEM((...]
where the time goes in v3:
time: 46.1 us; the launch traced here: 45.9 us
  Pallas kernels  45.1 us (98%)
  local copies, waits for them, and re-layouts  0.8 us (2%)
    pallas_call x1, Pallas kernels, kernel_body(): pl.pallas_call(functools.partial(kernel, scaling), out_shape=pltpu.VMEM((...  45.1 us

profile of v3, /device:TPU:1, one launch (start us, length us, event | category | flops | bytes accessed | tf_op | source)
XLA Modules:
  0.0 45.9 jit_solution(4651544497660588675)
XLA Ops:
  0.0 45.1 %shard_map.55 = bf16[512,512]{1,0:T(8,128)(2,1)S(1)} custom-call(bf16[512,2048]{1,0:T(8,128)(2,1)} %tok_hbm.1, bf16[2048,512]{1,0:T(8,128)(2,1)} %w_hbm.1, bf16[1024,512]{1,0:T(8,128)(2,1)} %constant.6.clone.high_hbm, bf16[1024,512]{1,0:T(8,128)(2,1)} %constant.7.clone.low_hbm, f32[512,128]{1,0:T(8,128)} %constant.8.clone.twist_hbm), custom_call_target="tpu_custom_call" | custom-call | tf_op jit(solution)/shard_map/pallas_call | solution.py:551
  45.2 0.8 %copy.7 = bf16[512,512]{1,0:T(8,128)(2,1)} copy(bf16[512,512]{1,0:T(8,128)(2,1)S(1)} %shard_map.55) | data formatting | bytes 1048576

commit v4 on v3

--- a/solution.py
+++ b/solution.py
@@ -472,7 +472,16 @@
             rows = slice(half * mid, (half + 1) * mid)
             high, low = split(jnp.concatenate(parts, axis=1))
             terms = dot(high, fold_high[at]) + dot(low, fold_high[at])
-            total[rows] += terms + dot(high, fold_low[at])
+            terms += dot(high, fold_low[at])
+
+            @pl.when(at < SLOTS - 1)
+            def _():
+                total[rows] += terms
+
+            @pl.when(at == SLOTS - 1)
+            def _():
+                out_ref[rows] = (total[rows] + terms).astype(jnp.bfloat16)
+
 
     def owns(at):
         return jnp.logical_and(at < SLOTS, jnp.logical_and(central, core == at % 2))
@@ -516,8 +525,6 @@
         @pl.when(owns(step + 1))
         def _():
             prepare(step + 1)
-
-    out_ref[...] = total[...].astype(jnp.bfloat16)
 
     @pl.loop(0, SLOTS)
     def _(at):

time: 46.1 us -> 46.3 us (level)
  no operation moved by 1% of the time
where the time goes in v4:
time: 46.3 us; the launch traced here: 46.1 us
  Pallas kernels  45.3 us (98%)
  local copies, waits for them, and re-layouts  0.8 us (2%)
    pallas_call x1, Pallas kernels, kernel_body(): pl.pallas_call(functools.partial(kernel, scaling), out_shape=pltpu.VMEM((...  45.3 us

profile of v4, /device:TPU:1, one launch (start us, length us, event | category | flops | bytes accessed | tf_op | source)
XLA Modules:
  0.0 46.1 jit_solution(9789553963230611859)
XLA Ops:
  0.0 45.3 %shard_map.55 = bf16[512,512]{1,0:T(8,128)(2,1)S(1)} custom-call(bf16[512,2048]{1,0:T(8,128)(2,1)} %tok_hbm.1, bf16[2048,512]{1,0:T(8,128)(2,1)} %w_hbm.1, bf16[1024,512]{1,0:T(8,128)(2,1)} %constant.6.clone.high_hbm, bf16[1024,512]{1,0:T(8,128)(2,1)} %constant.7.clone.low_hbm, f32[512,128]{1,0:T(8,128)} %constant.8.clone.twist_hbm), custom_call_target="tpu_custom_call" | custom-call | tf_op jit(solution)/shard_map/pallas_call | solution.py:558
  45.4 0.8 %copy.7 = bf16[512,512]{1,0:T(8,128)(2,1)} copy(bf16[512,512]{1,0:T(8,128)(2,1)S(1)} %shard_map.55) | data formatting | bytes 1048576
